TPU v7x, 32 devices: a whole 2x2x4 slice. The times are simulated.
32 devices in a mesh: kv: 4 (over z), tp: 8 (over y, x, core).
Axes of the slice: x: 2, y: 2, z: 4, core: 2. Of those that a mesh axis runs over, the one named last changes fastest.
Arguments:
- piece_tokens: bfloat16 [512, 2048], P('kv'), may hold values from -6 to 6
- dec_tokens: bfloat16 [8, 2048], P('kv'), may hold values from -6 to 6
- norm_gain: float32 [2048], replicated, may hold values from 0.1 to 1.9
- w_query_nope: bfloat16 [2048, 2048], P(None, 'tp'), may hold values from -0.125 to 0.125
- w_query_rope: bfloat16 [2048, 1024], P(None, 'tp'), may hold values from -0.125 to 0.125
- w_latent: bfloat16 [2048, 512], replicated, may hold values from -0.125 to 0.125
- w_key_rope: bfloat16 [2048, 64], replicated, may hold values from -0.125 to 0.125
- latent_gain: float32 [512], replicated, may hold values from 0.1 to 1.9
- w_key_up: bfloat16 [16, 128, 512], P('tp'), may hold values from -0.5 to 0.5
- w_value_up: bfloat16 [16, 512, 128], P('tp'), may hold values from -3 to 3
- w_out: bfloat16 [2048, 2048], P(None, 'tp'), may hold values from -0.25 to 0.25
- prompt_latent: bfloat16 [2048, 512], P('kv'), may hold values from -210 to 210
- prompt_rope: bfloat16 [2048, 64], P('kv'), may hold values from -6 to 6
- dec_latent: bfloat16 [8, 1024, 512], P('kv'), may hold values from -210 to 210
- dec_rope: bfloat16 [8, 1024, 64], P('kv'), may hold values from -6 to 6
- dec_lengths: int32 [8], P('kv'), may hold values from 1 to 1024, 4096 in all
Outputs:
- piece_out: bfloat16 [512, 2048], P('kv', 'tp')
- dec_out: bfloat16 [8, 2048], P('kv', 'tp')
Inputs may be any that keep to these rules, and one draw needn't show every extreme that they name: `dec_lengths`: every decoding sequence has at least one live cache slot, and some sequence has all 1024.
All inputs are finite; a program needn't handle non-finite values. No bound on the sum of `dec_lengths` on one device may be relied on, other than what follows from the above.
Results may differ from a plain program's by a relative error of at most 0.025.
Values may be sent and summed in bfloat16 or wider, within the bound.
No kernel may reach another device: no remote copies, remote signals or barrier semaphores. Data moves between devices by JAX's collectives and lax.ppermute only.
A program may use at most 128 MiB of HBM per device.

v0:
```python
import jax
import jax.numpy as jnp
from jax import lax
from jax.sharding import PartitionSpec as P

epsilon = 1e-06
rope_base = 10000.0
masked = -1e30


def normalize(values, gain_vec):
    mean_sq = jnp.mean(values * values, axis=-1, keepdims=True)
    return values * lax.rsqrt(mean_sq + epsilon) * gain_vec


def rotate(values, positions):
    half_dim = values.shape[-1] // 2
    frequency = rope_base ** (-jnp.arange(half_dim, dtype=jnp.float32) / half_dim)
    angles = (positions.astype(jnp.float32)[:, None] * frequency[None, :])[:, None, :]
    cosines = jnp.cos(angles)
    sine_values = jnp.sin(angles)
    front_half = values[..., :half_dim]
    back_half = values[..., half_dim:]
    return jnp.concatenate(
        [
            front_half * cosines - back_half * sine_values,
            front_half * sine_values + back_half * cosines,
        ],
        axis=-1,
    )


def rounded(values):
    return lax.optimization_barrier(values.astype(jnp.bfloat16)).astype(jnp.float32)


def project(
    tokens, positions, norm_gain, w_query_nope, w_query_rope, w_latent, w_key_rope, latent_gain
):
    row_count = tokens.shape[0]
    rope_dim = w_key_rope.shape[1]
    head_count = w_query_rope.shape[1] // rope_dim
    normed = normalize(tokens.astype(jnp.float32), norm_gain).astype(jnp.bfloat16)
    query_nope = jnp.dot(normed, w_query_nope, preferred_element_type=jnp.float32).astype(
        jnp.bfloat16
    )
    query_raw = jnp.dot(normed, w_query_rope, preferred_element_type=jnp.float32).reshape(
        row_count, head_count, rope_dim
    )
    query_rot = rotate(query_raw, positions).astype(jnp.bfloat16)
    latent = normalize(
        jnp.dot(normed, w_latent, preferred_element_type=jnp.float32), latent_gain
    ).astype(jnp.bfloat16)
    key_raw = jnp.dot(normed, w_key_rope, preferred_element_type=jnp.float32)[:, None, :]
    key_rot = rotate(key_raw, positions)[:, 0].astype(jnp.bfloat16)
    return (query_nope, query_rot, latent, key_rot)


def absorb(query_nope, w_key_up):
    head_count, nope_dim, _ = w_key_up.shape
    by_head = query_nope.reshape(query_nope.shape[0], head_count, nope_dim)
    return jnp.einsum("nhd,hdc->nhc", by_head, w_key_up, preferred_element_type=jnp.float32).astype(
        jnp.bfloat16
    )


def shards(
    piece_tokens,
    dec_tokens,
    norm_gain,
    w_query_nope,
    w_query_rope,
    w_latent,
    w_key_rope,
    latent_gain,
    w_key_up,
    w_value_up,
    w_out,
    prompt_latent,
    prompt_rope,
    dec_latent,
    dec_rope,
    dec_lengths,
):
    piece_rows = piece_tokens.shape[0]
    dec_rows = dec_tokens.shape[0]
    cached = prompt_latent.shape[0]
    head_count, latent_dim, value_dim = w_value_up.shape
    rope_dim = w_key_rope.shape[1]
    nope_width = w_query_nope.shape[1]
    score_scale = (w_key_up.shape[1] + rope_dim) ** (-0.5)
    block_index = lax.axis_index("kv")
    prompt_len = cached * lax.axis_size("kv")
    piece_offset = block_index * piece_rows
    positions = jnp.concatenate(
        [prompt_len + piece_offset + jnp.arange(piece_rows, dtype=jnp.int32), dec_lengths]
    )
    tokens = jnp.concatenate([piece_tokens, dec_tokens], axis=0)
    query_nope, query_rot, new_latent, new_rot = project(
        tokens, positions, norm_gain, w_query_nope, w_query_rope, w_latent, w_key_rope, latent_gain
    )
    key_latent = jnp.concatenate([prompt_latent, new_latent[:piece_rows]], axis=0)
    key_rot = jnp.concatenate([prompt_rope, new_rot[:piece_rows]], axis=0)
    column = jnp.arange(key_latent.shape[0], dtype=jnp.int32)
    key_place = piece_offset + column - cached
    rot_width = head_count * rope_dim
    piece_rot = query_rot[:piece_rows].reshape(piece_rows, rot_width)
    outgoing = jnp.concatenate([query_nope[:piece_rows], piece_rot], axis=1)
    shard_rows = lax.all_gather(outgoing, "kv", axis=0, tiled=True)
    row_count = shard_rows.shape[0]
    query_lat = absorb(shard_rows[:, :nope_width], w_key_up)
    query_rope = shard_rows[:, nope_width:].reshape(row_count, head_count, rope_dim)
    score_row_count = query_lat.shape[0]
    scores = (
        jnp.einsum("qhc,kc->qhk", query_lat, key_latent, preferred_element_type=jnp.float32)
        + jnp.einsum("qhr,kr->qhk", query_rope, key_rot, preferred_element_type=jnp.float32)
    ) * score_scale
    query_place = jnp.arange(score_row_count, dtype=jnp.int32)
    visible = (column[None, :] < cached) | (key_place[None, :] <= query_place[:, None])
    scores = jnp.where(visible[:, None, :], scores, masked)
    row_peak = lax.pmax(jnp.max(scores, axis=2).astype(jnp.bfloat16), "kv").astype(jnp.float32)
    weights = jnp.exp(scores - row_peak[:, :, None])
    weight_sum = jnp.sum(weights, axis=2)
    mixed_lat = jnp.einsum(
        "qhk,kc->qhc", weights.astype(jnp.bfloat16), key_latent, preferred_element_type=jnp.float32
    ).astype(jnp.bfloat16)
    partial_value = jnp.einsum(
        "qhc,hcv->qhv", mixed_lat, w_value_up, preferred_element_type=jnp.float32
    )
    all_rows = partial_value.shape[0]
    partial_value = rounded(partial_value).reshape(all_rows, head_count * value_dim)
    summed, denominator = (
        lax.psum_scatter(
            partial_value.astype(jnp.bfloat16), "kv", scatter_dimension=0, tiled=True
        ).astype(jnp.float32),
        lax.psum_scatter(
            weight_sum.astype(jnp.bfloat16), "kv", scatter_dimension=0, tiled=True
        ).astype(jnp.float32),
    )
    piece_attn = (
        summed.reshape(piece_rows, head_count, value_dim) / denominator[:, :, None]
    ).astype(jnp.bfloat16)
    dec_query = absorb(query_nope[piece_rows:], w_key_up)
    dec_rot = query_rot[piece_rows:]
    own_lat = new_latent[piece_rows:]
    own_rot = new_rot[piece_rows:]
    cache_scores = (
        jnp.einsum("bhc,bkc->bhk", dec_query, dec_latent, preferred_element_type=jnp.float32)
        + jnp.einsum("bhr,bkr->bhk", dec_rot, dec_rope, preferred_element_type=jnp.float32)
    ) * score_scale
    live_keys = (
        jnp.arange(dec_latent.shape[1], dtype=jnp.int32)[None, None, :] < dec_lengths[:, None, None]
    )
    cache_scores = jnp.where(live_keys, cache_scores, masked)
    own_scores = (
        jnp.einsum("bhc,bc->bh", dec_query, own_lat, preferred_element_type=jnp.float32)
        + jnp.einsum("bhr,br->bh", dec_rot, own_rot, preferred_element_type=jnp.float32)
    ) * score_scale
    dec_peak = jnp.maximum(jnp.max(cache_scores, axis=2), own_scores)
    cache_w = jnp.exp(cache_scores - dec_peak[:, :, None])
    own_w = jnp.exp(own_scores - dec_peak)
    dec_sum = jnp.sum(cache_w, axis=2) + own_w
    dec_mix = (
        jnp.einsum(
            "bhk,bkc->bhc",
            cache_w.astype(jnp.bfloat16),
            dec_latent,
            preferred_element_type=jnp.float32,
        )
        + rounded(own_w)[:, :, None] * own_lat.astype(jnp.float32)[:, None, :]
    ).astype(jnp.bfloat16)
    dec_value = rounded(
        jnp.einsum("bhc,hcv->bhv", dec_mix, w_value_up, preferred_element_type=jnp.float32)
    )
    dec_attn = (dec_value / dec_sum[:, :, None]).astype(jnp.bfloat16)
    attended = jnp.concatenate(
        [
            piece_attn.reshape(piece_rows, head_count * value_dim),
            dec_attn.reshape(dec_rows, head_count * value_dim),
        ],
        axis=0,
    )
    result = jnp.dot(
        lax.all_gather(attended, "tp", axis=1, tiled=True),
        w_out,
        preferred_element_type=jnp.float32,
    ).astype(jnp.bfloat16)
    return (result[:piece_rows], result[piece_rows:])


def solution(mesh):
    in_specs = (
        P("kv", None),
        P("kv", None),
        P(),
        P(None, "tp"),
        P(None, "tp"),
        P(),
        P(),
        P(),
        P("tp", None, None),
        P("tp", None, None),
        P(None, "tp"),
        P("kv", None),
        P("kv", None),
        P("kv", None, None),
        P("kv", None, None),
        P("kv"),
    )
    out_specs = (P("kv", "tp"), P("kv", "tp"))
    return jax.shard_map(shards, mesh=mesh, in_specs=in_specs, out_specs=out_specs, check_vma=False)
```

profile of v0, /device:TPU:0, one launch (start us, length us, event | category | flops | bytes accessed | tf_op | source)
XLA Modules:
  0.0 113.8 jit_solution(15459763306817569072)
XLA Ops:
  7.3 1.4 %fusion.16 = f32[130]{0:T(256)S(1)} fusion(bf16[2,2048]{1,0:T(2,128)(2,1)} %param.17, bf16[128,2048]{1,0:T(8,128)(2,1)} %param.16), kind=kLoop, calls=%fused_computation.19 | loop fusion | flops 1597310 | bytes 533000 | tf_op jit(solution)/shard_map/reduce_sum | solution.py:12
  8.7 1.9 %convolution_convert_fusion.3 = bf16[130,256]{1,0:T(8,128)(2,1)S(1)} fusion(bf16[2048,256]{1,0:T(8,128)(2,1)} %param.19, f32[2048]{0:T(1024)} %param.18, f32[130]{0:T(256)S(1)} %add_rsqrt_fusion.1, bf16[2,2048]{1,0:T(2,128)(2,1)} %param.17, bf16[128,2048]{1,0:T(8,128)(2,1)} %param.16), kind=kOutput, calls=%fused_computation.17 | convolution fusion | flops 138211840 | bytes 1656328 | tf_op jit(solution)/shard_map/dot_general | solution.py:44
  10.6 0.4 fusion.63
  11.0 0.1 reshape.229
  11.2 0.6 multiply_reduce_fusion
  11.8 0.3 copy-done.11
  12.1 0.4 convolution_bitcast_fusion
  12.6 0.3 multiply_cosine_fusion
  12.9 0.2 fusion.36
  13.1 0.1 multiply_convert_fusion
  13.3 0.3 subtract_convert_fusion
  13.6 0.2 pad_maximum_fusion.4
  13.8 0.1 copy.44
  13.9 0.1 copy.45
  14.0 16.3 %all_gather.6 = bf16[512,384]{1,0:T(8,128)(2,1)S(1)} all-gather(bf16[128,384]{1,0:T(8,128)(2,1)S(1)} %pad_maximum_fusion.2), channel_id=1, replica_groups=mesh['kv'=4,'tp'=8] {'kv'}, dimensions={0}, use_global_device_ids=true | all-gather | bytes 491520 | tf_op jit(solution)/shard_map/all_gather | solution.py:109
  30.3 0.8 copy.47
  31.1 0.2 fusion.9
  31.3 3.8 %fusion.3 = f32[512,2,640]{2,0,1:T(8,128)} fusion(bf16[2,128,512]{2,1,0:T(8,128)(2,1)S(1)} %copy-done.2, bf16[128,512]{1,0:T(8,128)(2,1)S(1)} %slice.76, bf16[512,512]{1,0:T(8,128)(2,1)} %param.27, bf16[512,384]{1,0:T(8,128)(2,1)S(1)} %all_gather.6), kind=kOutput, calls=%fused_computation.9 | convolution fusion | flops 807141376 | bytes 3801088 | tf_op jit(solution)/shard_map/qhc,kc->qhk/dot_general | solution.py:115
  35.1 4.2 %fusion.68 = (bf16[512,2]{0,1:T(2,128)(2,1)S(1)}, f32[512,2,640]{2,0,1:T(8,128)}) fusion(f32[512,2,640]{2,0,1:T(8,128)} %fusion.3, bf16[512,2,64]{0,2,1:T(8,128)(2,1)} %bitcast.72, bf16[128,64]{0,1:T(8,128)(2,1)S(1)} %fusion.40, bf16[512,64]{0,1:T(8,128)(2,1)} %param.28, pred[512,640]{1,0:T(8,128)(4,1)S(1)} %fusion.9), kind=kOutput, calls=%fused_computation.102 | convolution fusion | flops 86670336 | bytes 5785600 | tf_op jit(solution)/shard_map/qhr,kr->qhk/dot_general | solution.py:116
  39.3 12.4 %pmax.7 = bf16[512,2]{0,1:T(2,128)(2,1)S(1)} all-reduce(bf16[512,2]{0,1:T(2,128)(2,1)S(1)} %get-tuple-element.16), channel_id=1, replica_groups=mesh['kv'=4,'tp'=8] {'kv'}, use_global_device_ids=true, to_apply=%region_3.4 | all-reduce | flops 1024 | bytes 4096 | tf_op jit(solution)/shard_map/pmax | solution.py:121
  51.8 2.4 %fusion = bf16[512,2]{0,1:T(2,128)(2,1)S(1)} fusion(f32[512,2,640]{2,0,1:T(8,128)} %get-tuple-element.17, f32[512,2]{0,1:T(2,128)S(1)} %convert_element_type.109), kind=kLoop, calls=%fused_computation.2 | loop fusion | flops 1309696 | bytes 2627584 | tf_op jit(solution)/shard_map/reduce_sum | solution.py:123
  54.1 0.8 copy.61
  55.0 0.0 reduce-scatter.7.cloned.1.call-start
  55.0 3.8 %fusion.13 = bf16[512,2,128]{2,0,1:T(8,128)(2,1)} fusion(bf16[2,512,128]{2,1,0:T(8,128)(2,1)} %param.25, f32[512,2,640]{2,0,1:T(8,128)} %get-tuple-element.17, f32[512,2]{0,1:T(2,128)S(1)} %convert_element_type.109, bf16[128,512]{1,0:T(8,128)(2,1)S(1)} %slice.76, bf16[512,512]{1,0:T(8,128)(2,1)S(1)} %copy-done.4), kind=kOutput, calls=%fused_computation.15 | convolution fusion | flops 808583168 | bytes 3805184 | tf_op jit(solution)/shard_map/qhc,hcv->qhv/dot_general | solution.py:127
  58.9 1.1 copy.48
  59.9 0.8 copy.59
  60.8 0.9 fusion.22
  61.7 0.2 pad_maximum_fusion.3
  61.9 0.1 iota_compare_fusion.1
  62.0 2.2 %fusion.49 = f32[2,2,1024]{2,1,0:T(2,128)S(1)} fusion(bf16[2,1024,512]{2,1,0:T(8,128)(2,1)} %param.29, bf16[2,2,512]{2,0,1:T(2,128)(2,1)S(1)} %fusion.22), kind=kOutput, calls=%fused_computation.77 | convolution fusion | flops 4194304 | bytes 2117632 | tf_op jit(solution)/shard_map/bhc,bkc->bhk/dot_general | solution.py:148
  64.2 0.1 fusion.46
  64.3 0.1 copy.51
  64.4 0.1 fusion.53
  64.5 0.3 fusion.67
  64.8 0.2 fusion.41
  65.0 2.0 %fusion.21 = bf16[2,2,512]{2,1,0:T(2,128)(2,1)S(1)} fusion(bf16[2,1024,512]{2,1,0:T(8,128)(2,1)} %param.29, f32[2,2,1024]{2,1,0:T(2,128)S(1)} %get-tuple-element.13, f32[2,2]{1,0:T(2,128)S(1)} %fusion.55, f32[2,512]{1,0:T(2,128)S(1)} %get-tuple-element.6, f32[2,2]{1,0:T(2,128)S(1)} %convert_element_type.123), kind=kOutput, calls=%fused_computation.26 | convolution fusion | flops 4208640 | bytes 2121760 | tf_op jit(solution)/shard_map/bhk,bkc->bhc/dot_general | solution.py:164
  67.0 0.1 fusion.23
  67.2 0.1 copy.53
  67.3 0.1 fusion.52
  67.4 0.1 copy.54
  67.5 5.3 %reduce-scatter.9.cloned.1.call-done = bf16[128,2]{1,0:T(8,128)(2,1)} async-done(((bf16[512,2]{1,0:T(8,128)(2,1)}), bf16[128,2]{1,0:T(8,128)(2,1)}) %reduce-scatter.9.cloned.1.call-update) | async-done | bytes 528
  72.8 0.8 copy.62
  73.6 19.7 %reduce-scatter.7.cloned.1.call-done = bf16[128,256]{1,0:T(8,128)(2,1)} async-done(((bf16[512,256]{1,0:T(8,128)(2,1)}), bf16[128,256]{1,0:T(8,128)(2,1)}) %reduce-scatter.7.cloned.1.call-update) | async-done | bytes 65552
  93.3 0.9 copy.60
  94.3 10.9 %all_gather.7 = bf16[130,2048]{0,1:T(8,128)(2,1)S(1)} all-gather(bf16[130,256]{0,1:T(8,128)(2,1)S(1)} %pad_maximum_fusion.1), channel_id=1, replica_groups=mesh['kv'=4,'tp'=8] {'tp'}, dimensions={1}, use_global_device_ids=true | all-gather | bytes 599040 | tf_op jit(solution)/shard_map/all_gather | solution.py:184
  105.2 0.5 convolution_convert_fusion.2
  105.7 0.6 slice.84
  106.4 0.6 slice.85
  (51 shorter events, 0.3 us)
Async XLA Ops:
  7.2 4.0 %copy-start = (bf16[2048,512]{1,0:T(8,128)(2,1)S(1)}, bf16[2048,512]{1,0:T(8,128)(2,1)}, u32[]{:S(2)}) copy-start(bf16[2048,512]{1,0:T(8,128)(2,1)} %param.21) | copy-start | bytes 6291460
  7.2 65.6 %reduce-scatter.9.cloned.1.call-start = ((), (), s32[]{:S(2)}) async-start(), calls=%async_computation.3 | async-start | bytes 163840
  8.6 1.9 %copy-start.3 = (bf16[128,2048]{1,0:T(8,128)(2,1)S(1)}, bf16[128,2048]{1,0:T(8,128)(2,1)}, u32[]{:S(2)}) copy-start(bf16[128,2048]{1,0:T(8,128)(2,1)} %param.16) | copy-start | bytes 1572868
  8.7 1.9 %copy-start.7 = (bf16[2,2048]{1,0:T(2,128)(2,1)S(1)}, bf16[2,2048]{1,0:T(2,128)(2,1)}, u32[]{:S(2)}) copy-start(bf16[2,2048]{1,0:T(2,128)(2,1)} %param.17) | copy-start | bytes 24580
  8.7 1.9 %copy-start.10 = (bf16[2048,128]{1,0:T(8,128)(2,1)S(1)}, bf16[2048,128]{1,0:T(8,128)(2,1)}, u32[]{:S(2)}) copy-start(bf16[2048,128]{1,0:T(8,128)(2,1)} %param.20) | copy-start | bytes 1572868
  8.7 1.9 %copy-start.13 = (f32[2048]{0:T(1024)S(1)}, f32[2048]{0:T(1024)}, u32[]{:S(2)}) copy-start(f32[2048]{0:T(1024)} %param.18) | copy-start | bytes 24580
  10.6 3.4 %copy-start.6 = (bf16[130,256]{1,0:T(8,128)(2,1)}, bf16[130,256]{1,0:T(8,128)(2,1)S(1)}, u32[]{:S(2)}) copy-start(bf16[130,256]{1,0:T(8,128)(2,1)S(1)} %convolution_convert_fusion.3) | copy-start | bytes 199684
  11.2 1.0 copy-start.11
  11.8 0.8 copy-start.9
  11.8 1.3 %copy-start.8 = (f32[512]{0:T(512)S(1)}, f32[512]{0:T(512)}, u32[]{:S(2)}) copy-start(f32[512]{0:T(512)} %param.23) | copy-start | bytes 6148
  13.2 18.1 %copy-start.2 = (bf16[2,128,512]{2,1,0:T(8,128)(2,1)S(1)}, bf16[2,128,512]{2,1,0:T(8,128)(2,1)}, u32[]{:S(2)}) copy-start(bf16[2,128,512]{2,1,0:T(8,128)(2,1)} %param.24) | copy-start | bytes 786436
  51.7 3.3 %copy-start.4 = (bf16[512,512]{1,0:T(8,128)(2,1)S(1)}, bf16[512,512]{1,0:T(8,128)(2,1)}, u32[]{:S(2)}) copy-start(bf16[512,512]{1,0:T(8,128)(2,1)} %param.27) | copy-start | bytes 1572868
  55.0 38.3 %reduce-scatter.7.cloned.1.call-start = ((), (), s32[]{:S(2)}) async-start(), calls=%async_computation.2 | async-start | bytes 327680
  60.8 3.7 %copy-start.12 = (bf16[2,1024,64]{1,2,0:T(8,128)(2,1)S(1)}, bf16[2,1024,64]{1,2,0:T(8,128)(2,1)}, u32[]{:S(2)}) copy-start(bf16[2,1024,64]{1,2,0:T(8,128)(2,1)} %param.30) | copy-start | bytes 786436
  64.2 2.8 %copy-start.5 = (bf16[2,512,128]{2,1,0:T(8,128)(2,1)S(1)}, bf16[2,512,128]{2,1,0:T(8,128)(2,1)}, u32[]{:S(2)}) copy-start(bf16[2,512,128]{2,1,0:T(8,128)(2,1)} %param.25) | copy-start | bytes 786436
  67.0 38.2 %copy-start.1 = (bf16[2048,256]{1,0:T(8,128)(2,1)S(1)}, bf16[2048,256]{1,0:T(8,128)(2,1)}, u32[]{:S(2)}) copy-start(bf16[2048,256]{1,0:T(8,128)(2,1)} %param.26) | copy-start | bytes 3145732
Sparse Core Ops, SparseCore 0:
  55.1 17.6 reduce-scatter.8
  75.1 18.2 reduce-scatter.6
where the time goes:
time: 114 us
  blocking collectives  39.6 us (35%)
  waiting for transfers between devices  25 us (22%)
  matrix products  21.3 us (19%)
  between operations  14.4 us (13%)
  local copies, waits for them, and re-layouts  7.52 us (7%)
  other arithmetic  5.78 us (5%)
    unnamed x4, waiting for transfers between devices  25 us
    all_gather x1, blocking collectives, shards(): shard_rows = lax.all_gather(outgoing, 'kv', axis=0, tiled=True)  16.3 us
    pmax x1, blocking collectives, shards(): lax.pmax(jnp.max(scores, axis=2).astype(jnp.bfloat16), 'kv')  12.4 us
    all_gather x1, blocking collectives, shards(): lax.all_gather(attended, 'tp', axis=1, tiled=True)  10.9 us
    dot_general x1, matrix products, shards(): jnp.einsum('qhr,kr->qhk', query_rope, key_rot, preferred_element_type=jnp...  4.18 us
    dot_general x1, matrix products, shards(): jnp.einsum('qhc,hcv->qhv', mixed_lat, w_value_up, preferred_element_type=...  3.83 us
    dot_general x1, matrix products, shards(): jnp.einsum('qhc,kc->qhk', query_lat, key_latent, preferred_element_type=j...  3.79 us
    unnamed x32, local copies, waits for them, and re-layouts  3.78 us
  transfers between devices with their start and end apart: 2, of which 2 were waited for; matrix products, arithmetic and copies ran while one was open for 12% of the time, Pallas kernels for 0%

commit v1 on v0

--- a/solution.py
+++ b/solution.py
@@ -6,6 +6,12 @@
 epsilon = 1e-06
 rope_base = 10000.0
 masked = -1e30
+
+
+def all_parts(block, mesh_axis, dim):
+    terms = lax.all_gather(block, mesh_axis, axis=0, tiled=False)
+    whole = jnp.concatenate(terms, axis=dim)
+    return whole
 
 
 def normalize(values, gain_vec):
@@ -181,9 +187,7 @@
         axis=0,
     )
     result = jnp.dot(
-        lax.all_gather(attended, "tp", axis=1, tiled=True),
-        w_out,
-        preferred_element_type=jnp.float32,
+        all_parts(attended, "tp", 1), w_out, preferred_element_type=jnp.float32
     ).astype(jnp.bfloat16)
     return (result[:piece_rows], result[piece_rows:])
 

time: 114 us -> 115 us (level)
  local copies, waits for them, and re-layouts: 7.52 us -> 8.92 us
    unnamed x32 -> x35, local copies, waits for them, and re-layouts: 3.78 us -> 5.08 us
where the time goes in v1:
time: 115 us; the launch traced here: 114 us
  blocking collectives  38.6 us (34%)
  waiting for transfers between devices  25.1 us (22%)
  matrix products  21.2 us (18%)
  between operations  14.5 us (13%)
  local copies, waits for them, and re-layouts  8.92 us (8%)
  other arithmetic  5.78 us (5%)
    unnamed x4, waiting for transfers between devices  25.1 us
    all_gather x1, blocking collectives, shards(): shard_rows = lax.all_gather(outgoing, 'kv', axis=0, tiled=True)  16.3 us
    pmax x1, blocking collectives, shards(): lax.pmax(jnp.max(scores, axis=2).astype(jnp.bfloat16), 'kv')  12.4 us
    all_gather x1, blocking collectives, all_parts(): terms = lax.all_gather(block, mesh_axis, axis=0, tiled=False)  9.93 us
    unnamed x35, local copies, waits for them, and re-layouts  5.08 us
    dot_general x1, matrix products, shards(): jnp.einsum('qhr,kr->qhk', query_rope, key_rot, preferred_element_type=jnp...  4.18 us
    dot_general x1, matrix products, shards(): jnp.einsum('qhc,hcv->qhv', mixed_lat, w_value_up, preferred_element_type=...  3.83 us
    dot_general x1, matrix products, shards(): jnp.einsum('qhc,kc->qhk', query_lat, key_latent, preferred_element_type=j...  3.79 us
  transfers between devices with their start and end apart: 2, of which 2 were waited for; matrix products, arithmetic and copies ran while one was open for 12% of the time, Pallas kernels for 0%

profile of v1, /device:TPU:0, one launch (start us, length us, event | category | flops | bytes accessed | tf_op | source)
XLA Modules:
  0.0 114.2 jit_solution(14728561092773755807)
XLA Ops:
  7.3 1.4 %fusion.16 = f32[130]{0:T(256)S(1)} fusion(bf16[2,2048]{1,0:T(2,128)(2,1)} %param.17, bf16[128,2048]{1,0:T(8,128)(2,1)} %param.16), kind=kLoop, calls=%fused_computation.19 | loop fusion | flops 1597310 | bytes 533000 | tf_op jit(solution)/shard_map/reduce_sum | solution.py:18
  8.7 1.9 %convolution_convert_fusion.3 = bf16[130,256]{1,0:T(8,128)(2,1)S(1)} fusion(bf16[2048,256]{1,0:T(8,128)(2,1)} %param.19, f32[2048]{0:T(1024)} %param.18, f32[130]{0:T(256)S(1)} %add_rsqrt_fusion.1, bf16[2,2048]{1,0:T(2,128)(2,1)} %param.17, bf16[128,2048]{1,0:T(8,128)(2,1)} %param.16), kind=kOutput, calls=%fused_computation.17 | convolution fusion | flops 138211840 | bytes 1656328 | tf_op jit(solution)/shard_map/dot_general | solution.py:50
  10.6 0.4 fusion.63
  11.0 0.1 reshape.235
  11.2 0.6 multiply_reduce_fusion
  11.8 0.3 copy-done.11
  12.1 0.4 convolution_bitcast_fusion
  12.6 0.3 multiply_cosine_fusion
  12.9 0.2 fusion.36
  13.1 0.1 multiply_convert_fusion
  13.3 0.3 subtract_convert_fusion
  13.6 0.2 pad_maximum_fusion.3
  13.8 0.1 copy.46
  13.9 0.1 copy.47
  14.0 16.3 %all_gather.9 = bf16[512,384]{1,0:T(8,128)(2,1)S(1)} all-gather(bf16[128,384]{1,0:T(8,128)(2,1)S(1)} %pad_maximum_fusion.1), channel_id=1, replica_groups=mesh['kv'=4,'tp'=8] {'kv'}, dimensions={0}, use_global_device_ids=true | all-gather | bytes 491520 | tf_op jit(solution)/shard_map/all_gather | solution.py:115
  30.3 0.8 copy.49
  31.1 0.2 fusion.9
  31.3 3.8 %fusion.3 = f32[512,2,640]{2,0,1:T(8,128)} fusion(bf16[2,128,512]{2,1,0:T(8,128)(2,1)S(1)} %copy-done.2, bf16[128,512]{1,0:T(8,128)(2,1)S(1)} %slice.76, bf16[512,512]{1,0:T(8,128)(2,1)} %param.27, bf16[512,384]{1,0:T(8,128)(2,1)S(1)} %all_gather.9), kind=kOutput, calls=%fused_computation.9 | convolution fusion | flops 807141376 | bytes 3801088 | tf_op jit(solution)/shard_map/qhc,kc->qhk/dot_general | solution.py:121
  35.1 4.2 %fusion.68 = (bf16[512,2]{0,1:T(2,128)(2,1)S(1)}, f32[512,2,640]{2,0,1:T(8,128)}) fusion(f32[512,2,640]{2,0,1:T(8,128)} %fusion.3, bf16[512,2,64]{0,2,1:T(8,128)(2,1)} %bitcast.81, bf16[128,64]{0,1:T(8,128)(2,1)S(1)} %fusion.40, bf16[512,64]{0,1:T(8,128)(2,1)} %param.28, pred[512,640]{1,0:T(8,128)(4,1)S(1)} %fusion.9), kind=kOutput, calls=%fused_computation.102 | convolution fusion | flops 86670336 | bytes 5785600 | tf_op jit(solution)/shard_map/qhr,kr->qhk/dot_general | solution.py:122
  39.3 12.4 %pmax.7 = bf16[512,2]{0,1:T(2,128)(2,1)S(1)} all-reduce(bf16[512,2]{0,1:T(2,128)(2,1)S(1)} %get-tuple-element.16), channel_id=1, replica_groups=mesh['kv'=4,'tp'=8] {'kv'}, use_global_device_ids=true, to_apply=%region_3.4 | all-reduce | flops 1024 | bytes 4096 | tf_op jit(solution)/shard_map/pmax | solution.py:127
  51.8 2.4 %fusion = bf16[512,2]{0,1:T(2,128)(2,1)S(1)} fusion(f32[512,2,640]{2,0,1:T(8,128)} %get-tuple-element.17, f32[512,2]{0,1:T(2,128)S(1)} %convert_element_type.109), kind=kLoop, calls=%fused_computation.2 | loop fusion | flops 1309696 | bytes 2627584 | tf_op jit(solution)/shard_map/reduce_sum | solution.py:129
  54.1 0.8 copy.65
  55.0 3.8 %fusion.13 = bf16[512,2,128]{2,0,1:T(8,128)(2,1)} fusion(bf16[2,512,128]{2,1,0:T(8,128)(2,1)} %param.25, f32[512,2,640]{2,0,1:T(8,128)} %get-tuple-element.17, f32[512,2]{0,1:T(2,128)S(1)} %convert_element_type.109, bf16[128,512]{1,0:T(8,128)(2,1)S(1)} %slice.76, bf16[512,512]{1,0:T(8,128)(2,1)S(1)} %copy-done.4), kind=kOutput, calls=%fused_computation.15 | convolution fusion | flops 808583168 | bytes 3805184 | tf_op jit(solution)/shard_map/qhc,hcv->qhv/dot_general | solution.py:133
  58.9 1.1 copy.50
  59.9 0.8 copy.63
  60.8 0.9 fusion.22
  61.7 0.2 pad_maximum_fusion.2
  62.0 2.2 %fusion.49 = f32[2,2,1024]{2,1,0:T(2,128)S(1)} fusion(bf16[2,1024,512]{2,1,0:T(8,128)(2,1)} %param.29, bf16[2,2,512]{2,0,1:T(2,128)(2,1)S(1)} %fusion.22), kind=kOutput, calls=%fused_computation.77 | convolution fusion | flops 4194304 | bytes 2117632 | tf_op jit(solution)/shard_map/bhc,bkc->bhk/dot_general | solution.py:154
  64.2 0.1 fusion.46
  64.4 0.1 fusion.53
  64.5 0.3 fusion.67
  64.8 0.2 fusion.41
  65.0 2.0 %fusion.21 = bf16[2,2,512]{2,1,0:T(2,128)(2,1)S(1)} fusion(bf16[2,1024,512]{2,1,0:T(8,128)(2,1)} %param.29, f32[2,2,1024]{2,1,0:T(2,128)S(1)} %get-tuple-element.13, f32[2,2]{1,0:T(2,128)S(1)} %fusion.55, f32[2,512]{1,0:T(2,128)S(1)} %get-tuple-element.6, f32[2,2]{1,0:T(2,128)S(1)} %convert_element_type.123), kind=kOutput, calls=%fused_computation.26 | convolution fusion | flops 4208640 | bytes 2121760 | tf_op jit(solution)/shard_map/bhk,bkc->bhc/dot_general | solution.py:170
  67.0 0.2 fusion.23
  67.2 0.1 copy.55
  67.4 0.1 copy.56
  67.5 5.3 %reduce-scatter.9.cloned.1.call-done = bf16[128,2]{1,0:T(8,128)(2,1)} async-done(((bf16[512,2]{1,0:T(8,128)(2,1)}), bf16[128,2]{1,0:T(8,128)(2,1)}) %reduce-scatter.9.cloned.1.call-update) | async-done | bytes 528
  72.8 0.8 copy.66
  73.6 19.8 %reduce-scatter.7.cloned.1.call-done = bf16[128,256]{1,0:T(8,128)(2,1)} async-done(((bf16[512,256]{1,0:T(8,128)(2,1)}), bf16[128,256]{1,0:T(8,128)(2,1)}) %reduce-scatter.7.cloned.1.call-update) | async-done | bytes 65552
  93.4 0.9 copy.64
  94.4 0.1 copy.57
  94.5 9.9 %all-gather.1 = bf16[8,130,256]{2,1,0:T(8,128)(2,1)S(1)} all-gather(bf16[1,130,256]{2,1,0:T(8,128)(2,1)S(1)} %copy.57), channel_id=2, replica_groups=mesh['kv'=4,'tp'=8] {'tp'}, dimensions={0}, use_global_device_ids=true | all-gather | bytes 599040 | tf_op jit(solution)/shard_map/all_gather | solution.py:12
  104.5 0.1 copy.58
  104.6 0.1 copy.68
  104.8 1.0 copy-done.1
  105.8 0.3 convolution_convert_fusion.2
  106.1 0.6 slice.84
  106.8 0.6 slice.85
  (55 shorter events, 0.6 us)
Async XLA Ops:
  7.2 4.0 %copy-start = (bf16[2048,512]{1,0:T(8,128)(2,1)S(1)}, bf16[2048,512]{1,0:T(8,128)(2,1)}, u32[]{:S(2)}) copy-start(bf16[2048,512]{1,0:T(8,128)(2,1)} %param.21) | copy-start | bytes 6291460
  7.2 65.6 %reduce-scatter.9.cloned.1.call-start = ((), (), s32[]{:S(2)}) async-start(), calls=%async_computation.3 | async-start | bytes 163840
  8.6 1.9 %copy-start.3 = (bf16[128,2048]{1,0:T(8,128)(2,1)S(1)}, bf16[128,2048]{1,0:T(8,128)(2,1)}, u32[]{:S(2)}) copy-start(bf16[128,2048]{1,0:T(8,128)(2,1)} %param.16) | copy-start | bytes 1572868
  8.7 1.9 %copy-start.7 = (bf16[2,2048]{1,0:T(2,128)(2,1)S(1)}, bf16[2,2048]{1,0:T(2,128)(2,1)}, u32[]{:S(2)}) copy-start(bf16[2,2048]{1,0:T(2,128)(2,1)} %param.17) | copy-start | bytes 24580
  8.7 1.9 %copy-start.10 = (bf16[2048,128]{1,0:T(8,128)(2,1)S(1)}, bf16[2048,128]{1,0:T(8,128)(2,1)}, u32[]{:S(2)}) copy-start(bf16[2048,128]{1,0:T(8,128)(2,1)} %param.20) | copy-start | bytes 1572868
  8.7 1.9 %copy-start.13 = (f32[2048]{0:T(1024)S(1)}, f32[2048]{0:T(1024)}, u32[]{:S(2)}) copy-start(f32[2048]{0:T(1024)} %param.18) | copy-start | bytes 24580
  10.6 3.4 %copy-start.6 = (bf16[130,256]{1,0:T(8,128)(2,1)}, bf16[130,256]{1,0:T(8,128)(2,1)S(1)}, u32[]{:S(2)}) copy-start(bf16[130,256]{1,0:T(8,128)(2,1)S(1)} %convolution_convert_fusion.3) | copy-start | bytes 199684
  11.2 1.0 copy-start.11
  11.8 0.8 copy-start.9
  11.8 1.3 %copy-start.8 = (f32[512]{0:T(512)S(1)}, f32[512]{0:T(512)}, u32[]{:S(2)}) copy-start(f32[512]{0:T(512)} %param.23) | copy-start | bytes 6148
  13.2 18.1 %copy-start.2 = (bf16[2,128,512]{2,1,0:T(8,128)(2,1)S(1)}, bf16[2,128,512]{2,1,0:T(8,128)(2,1)}, u32[]{:S(2)}) copy-start(bf16[2,128,512]{2,1,0:T(8,128)(2,1)} %param.24) | copy-start | bytes 786436
  51.7 3.3 %copy-start.4 = (bf16[512,512]{1,0:T(8,128)(2,1)S(1)}, bf16[512,512]{1,0:T(8,128)(2,1)}, u32[]{:S(2)}) copy-start(bf16[512,512]{1,0:T(8,128)(2,1)} %param.27) | copy-start | bytes 1572868
  55.0 38.5 %reduce-scatter.7.cloned.1.call-start = ((), (), s32[]{:S(2)}) async-start(), calls=%async_computation.2 | async-start | bytes 327680
  60.8 3.7 %copy-start.12 = (bf16[2,1024,64]{1,2,0:T(8,128)(2,1)S(1)}, bf16[2,1024,64]{1,2,0:T(8,128)(2,1)}, u32[]{:S(2)}) copy-start(bf16[2,1024,64]{1,2,0:T(8,128)(2,1)} %param.30) | copy-start | bytes 786436
  64.2 2.8 %copy-start.5 = (bf16[2,512,128]{2,1,0:T(8,128)(2,1)S(1)}, bf16[2,512,128]{2,1,0:T(8,128)(2,1)}, u32[]{:S(2)}) copy-start(bf16[2,512,128]{2,1,0:T(8,128)(2,1)} %param.25) | copy-start | bytes 786436
  104.6 1.2 %copy-start.1 = (bf16[2048,256]{1,0:T(8,128)(2,1)S(1)}, bf16[2048,256]{1,0:T(8,128)(2,1)}, u32[]{:S(2)}) copy-start(bf16[2048,256]{1,0:T(8,128)(2,1)} %param.26) | copy-start | bytes 3145732
Sparse Core Ops, SparseCore 0:
  55.1 17.6 reduce-scatter.8
  75.1 18.3 reduce-scatter.6
